TPU v7x, 32 devices: a whole 2x2x4 slice. The times are simulated.
32 devices in a mesh: rep: 2 (over y), fs: 4 (over z), tp: 4 (over x, core).
Axes of the slice: x: 2, y: 2, z: 4, core: 2. Of those that a mesh axis runs over, the one named last changes fastest.
Arguments:
- tokens: bfloat16 [4096, 2048], P(('rep', 'fs'), 'tp'), may hold values from -6 to 6
- pre_gain: float32 [2048], replicated, may hold values from 0.1 to 1.9
- u_weight: float32 [2048, 512], P('fs', 'tp'), may hold values from -0.125 to 0.125
- u_scale: float32 [512], P('tp'), may hold values from 0.5 to 2
- v_weight: float32 [2048, 512], P('fs', 'tp'), may hold values from -0.125 to 0.125
- v_scale: float32 [512], P('tp'), may hold values from 0.5 to 2
- group_gain: float32 [512], P('tp'), may hold values from 0.1 to 1.9
- span_weight: bfloat16 [8, 128, 128], P('tp'), may hold values from -0.5 to 0.5
- span_bias: float32 [8, 128], P('tp'), may hold values from 0.5 to 1.5
- out_weight: float32 [512, 2048], P('tp', 'fs'), may hold values from -0.25 to 0.25
- out_scale: float32 [2048], P('fs'), may hold values from 0.5 to 2
- ffn_gain: float32 [2048], replicated, may hold values from 0.1 to 1.9
- gate_weight: float32 [2048, 5632], P('fs', 'tp'), may hold values from -0.125 to 0.125
- gate_scale: float32 [5632], P('tp'), may hold values from 0.5 to 2
- up_weight: float32 [2048, 5632], P('fs', 'tp'), may hold values from -0.125 to 0.125
- up_scale: float32 [5632], P('tp'), may hold values from 0.5 to 2
- down_weight: float32 [5632, 2048], P('tp', 'fs'), may hold values from -0.078125 to 0.078125
- down_scale: float32 [2048], P('fs'), may hold values from 0.5 to 2
Outputs:
- layer_out: bfloat16 [4096, 2048], P(('rep', 'fs'), 'tp')
All inputs are finite; a program needn't handle non-finite values.
Results may differ from a plain program's by a relative error of at most 0.02.
Values may be sent and summed in bfloat16 or wider, within the bound.
A program may use at most 64 MiB of HBM per device.

v0:
```python
import jax
import jax.numpy as jnp
from jax import lax
from jax.sharding import PartitionSpec as P

EPS = 0.02


def rms_rows(values, gain):
    wide = values.astype(jnp.float32)
    scaled = wide * lax.rsqrt(jnp.mean(wide * wide, axis=-1, keepdims=True) + EPS)
    return (scaled * gain).astype(jnp.bfloat16)


def fold_pair(source, pieces):
    first = jnp.dot(source, pieces[0], preferred_element_type=jnp.float32)
    second = jnp.dot(source, pieces[1], preferred_element_type=jnp.float32)
    return (first, second)


def project_cols(source, scale_whole, piece):
    return jnp.dot(source, piece, preferred_element_type=jnp.float32) * scale_whole


def shards(
    tokens,
    pre_gain,
    u_weight,
    u_scale,
    v_weight,
    v_scale,
    group_gain,
    span_weight,
    span_bias,
    out_weight,
    out_scale,
    ffn_gain,
    gate_weight,
    gate_scale,
    up_weight,
    up_scale,
    down_weight,
    down_scale,
):
    gate_cast = gate_weight.astype(jnp.bfloat16)
    up_cast = up_weight.astype(jnp.bfloat16)
    full_rows = lax.all_gather(tokens, "tp", axis=1, tiled=True)
    row_count = full_rows.shape[0]
    normed = rms_rows(full_rows, pre_gain)
    u_pre, v_pre = fold_pair(
        normed,
        (
            lax.all_gather(u_weight.astype(jnp.bfloat16), "fs", axis=0, tiled=True),
            lax.all_gather(v_weight.astype(jnp.bfloat16), "fs", axis=0, tiled=True),
        ),
    )
    out_whole, down_whole = (
        lax.all_gather(out_scale, "fs", axis=0, tiled=True),
        lax.all_gather(down_scale, "fs", axis=0, tiled=True),
    )
    u_act = jax.nn.gelu(u_pre * u_scale)
    v_act = jax.nn.gelu(v_pre * v_scale)
    local_groups = span_weight.shape[0]
    span_len = span_weight.shape[1]
    group_width = v_act.shape[1] // local_groups
    grouped = v_act.reshape(row_count, local_groups, group_width)
    centre = jnp.mean(grouped, axis=-1, keepdims=True)
    spread = jnp.mean(jnp.square(grouped - centre), axis=-1, keepdims=True)
    v_norm = (
        ((grouped - centre) * lax.rsqrt(spread + EPS)).reshape(row_count, -1) * group_gain
    ).astype(jnp.bfloat16)
    spans = v_norm.reshape(row_count // span_len, span_len, local_groups, group_width)
    mixed = jnp.einsum(
        "gts,nsgc->ntgc", jnp.tril(span_weight), spans, preferred_element_type=jnp.float32
    )
    mixed = mixed + jnp.transpose(span_bias)[None, :, :, None]
    gated = (u_act * mixed.reshape(row_count, -1)).astype(jnp.bfloat16)
    out_cast = out_weight.astype(jnp.bfloat16)
    own_width = tokens.shape[1]
    gated_full = lax.all_gather(gated, "tp", axis=1, tiled=True)
    out_rows = lax.all_gather(out_cast, "fs", axis=1, tiled=True)
    out_own = lax.all_to_all(out_rows, "tp", split_axis=1, concat_axis=0, tiled=True)
    scale_own = lax.dynamic_slice_in_dim(out_whole, lax.axis_index("tp") * own_width, own_width, 0)
    mix_own = (jnp.dot(gated_full, out_own, preferred_element_type=jnp.float32) * scale_own).astype(
        jnp.bfloat16
    )
    resid_own = (tokens.astype(jnp.float32) + mix_own.astype(jnp.float32)).astype(jnp.bfloat16)
    resid_full = lax.all_gather(resid_own, "tp", axis=1, tiled=True)
    normed_ffn = rms_rows(resid_full, ffn_gain)
    gate_acc, up_acc = fold_pair(
        normed_ffn,
        (
            lax.all_gather(gate_cast, "fs", axis=0, tiled=True),
            lax.all_gather(up_cast, "fs", axis=0, tiled=True),
        ),
    )
    hidden = (jax.nn.silu(gate_acc * gate_scale) * (up_acc * up_scale)).astype(jnp.bfloat16)
    ffn_terms = project_cols(
        hidden,
        down_whole,
        lax.all_gather(down_weight.astype(jnp.bfloat16), "fs", axis=1, tiled=True),
    )
    ffn_own = lax.psum_scatter(
        ffn_terms.astype(jnp.bfloat16), "tp", scatter_dimension=1, tiled=True
    )
    return (resid_own.astype(jnp.float32) + ffn_own.astype(jnp.float32)).astype(jnp.bfloat16)


def solution(mesh):
    placed = (
        P(("rep", "fs"), "tp"),
        P(),
        P("fs", "tp"),
        P("tp"),
        P("fs", "tp"),
        P("tp"),
        P("tp"),
        P("tp", None, None),
        P("tp", None),
        P("tp", "fs"),
        P("fs"),
        P(),
        P("fs", "tp"),
        P("tp"),
        P("fs", "tp"),
        P("tp"),
        P("tp", "fs"),
        P("fs"),
    )
    return jax.shard_map(
        shards, mesh=mesh, in_specs=placed, out_specs=P(("rep", "fs"), "tp"), check_vma=False
    )
```

profile of v0, /device:TPU:0, one launch (start us, length us, event | category | flops | bytes accessed | tf_op | source)
XLA Modules:
  0.0 488.0 jit_solution(6885107651366701003)
XLA Ops:
  7.3 1.1 copy.48
  8.3 18.0 %all_gather.37 = bf16[128,2048]{0,1:T(8,128)(2,1)} all-gather(bf16[128,512]{0,1:T(8,128)(2,1)S(1)} %copy.48), channel_id=1, replica_groups=mesh['rep'=2,'fs'=4,'tp'=4] {'fs'}, dimensions={1}, use_global_device_ids=true | all-gather | bytes 655360 | tf_op jit(solution)/shard_map/all_gather | solution.py:81
  26.3 3.5 all-to-all-start
  30.9 12.3 %all-gather = f32[4,1,512]{2,1,0:T(1,128)S(1)} all-gather(f32[1,1,512]{2,1,0:T(1,128)S(1)} %bitcast.39), channel_id=1, replica_groups=mesh['rep'=2,'fs'=4,'tp'=4] {'fs'}, dimensions={0}, use_global_device_ids=true | all-gather | bytes 10240 | tf_op jit(solution)/shard_map/all_gather | solution.py:58
  43.4 16.0 %all_gather.35 = bf16[2048,128]{1,0:T(8,128)(2,1)S(1)} all-gather(bf16[512,128]{1,0:T(8,128)(2,1)S(1)} %convert_element_type.67), channel_id=1, replica_groups=mesh['rep'=2,'fs'=4,'tp'=4] {'fs'}, dimensions={0}, use_global_device_ids=true | all-gather | bytes 655360 | tf_op jit(solution)/shard_map/all_gather | solution.py:54
  59.4 15.9 %all_gather.34 = bf16[2048,128]{1,0:T(8,128)(2,1)} all-gather(bf16[512,128]{1,0:T(8,128)(2,1)S(1)} %convert_element_type.66), channel_id=1, replica_groups=mesh['rep'=2,'fs'=4,'tp'=4] {'fs'}, dimensions={0}, use_global_device_ids=true | all-gather | bytes 655360 | tf_op jit(solution)/shard_map/all_gather | solution.py:53
  76.3 2.1 fusion
  78.4 2.4 fusion.39
  82.5 1.9 fusion.30
  84.5 8.4 %all_gather.36 = bf16[512,512]{1,0:T(8,128)(2,1)S(1)} all-gather(bf16[512,128]{1,0:T(8,128)(2,1)S(1)} %fusion.30), channel_id=1, replica_groups=mesh['rep'=2,'fs'=4,'tp'=4] {'tp'}, dimensions={1}, use_global_device_ids=true | all-gather | bytes 655360 | tf_op jit(solution)/shard_map/all_gather | solution.py:80
  92.8 1.2 fusion.11
  94.2 1.3 convert_element_type.77
  95.5 3.3 convert_element_type.78
  98.9 1.4 convert_element_type.80
  100.3 12.1 %all-gather.1 = f32[4,1,512]{2,1,0:T(1,128)S(1)} all-gather(f32[1,1,512]{2,1,0:T(1,128)S(1)} %bitcast.40), channel_id=1, replica_groups=mesh['rep'=2,'fs'=4,'tp'=4] {'fs'}, dimensions={0}, use_global_device_ids=true | all-gather | bytes 10240 | tf_op jit(solution)/shard_map/all_gather | solution.py:59
  112.5 2.5 all-gather.10.cloned.1.call-done
  115.0 2.1 fusion.3
  117.1 106.2 %all-gather.12.cloned.1.call-done = bf16[2048,1408]{1,0:T(8,128)(2,1)} async-done(((bf16[512,1408]{1,0:T(8,128)(2,1)}), bf16[2048,1408]{1,0:T(8,128)(2,1)}) %all-gather.12.cloned.1.call-update) | async-done | bytes 5767184 | tf_op jit(solution)/shard_map/all_gather | solution.py:93
  223.3 8.3 %convolution_multiply_fusion.1 = f32[512,1408]{1,0:T(8,128)} fusion(bf16[2048,1408]{1,0:T(8,128)(2,1)} %all-gather.12.cloned.1.call-done, f32[1408]{0:T(1024)S(1)} %copy-done.14, bf16[512,2048]{1,0:T(8,128)(2,1)} %all-gather.10.cloned.1.call-done, f32[2048]{0:T(1024)S(1)} %copy-done.15, f32[512]{0:T(512)S(1)} %add_rsqrt_fusion.1), kind=kOutput, calls=%fused_computation.13 | convolution fusion | flops 2957705216 | bytes 10763776 | tf_op jit(solution)/shard_map/dot_general | solution.py:16
  231.6 98.1 %all-gather.14.cloned.1.call-done = bf16[2048,1408]{1,0:T(8,128)(2,1)} async-done(((bf16[512,1408]{1,0:T(8,128)(2,1)}), bf16[2048,1408]{1,0:T(8,128)(2,1)}) %all-gather.14.cloned.1.call-update) | async-done | bytes 5767184 | tf_op jit(solution)/shard_map/all_gather | solution.py:94
  329.7 106.4 %all-gather.16.cloned.1.call-done = bf16[1408,2048]{1,0:T(8,128)(2,1)} async-done(((bf16[1408,512]{1,0:T(8,128)(2,1)}), bf16[1408,2048]{1,0:T(8,128)(2,1)}) %all-gather.16.cloned.1.call-update) | async-done | bytes 5767184 | tf_op jit(solution)/shard_map/all_gather | solution.py:101
  436.1 13.5 %multiply_convert_fusion = bf16[512,2048]{1,0:T(8,128)(2,1)} fusion(bf16[1408,2048]{1,0:T(8,128)(2,1)} %all-gather.16.cloned.1.call-done, f32[2048]{0:T(1024)S(1)} %bitcast.38, bf16[2048,1408]{1,0:T(8,128)(2,1)} %all-gather.14.cloned.1.call-done, f32[512,1408]{1,0:T(8,128)} %convolution_multiply_fusion.1, f32[1408]{0:T(1024)S(1)} %copy-done.16, ...), kind=kOutput, calls=%fused_computation.10 | convolution fusion | flops 5916917760 | bytes 18636288 | tf_op jit(solution)/shard_map/dot_general | solution.py:22
  449.6 29.6 %reduce-scatter.2.cloned.1.call-done = bf16[512,512]{1,0:T(8,128)(2,1)} async-done(((bf16[512,2048]{1,0:T(8,128)(2,1)}), bf16[512,512]{1,0:T(8,128)(2,1)}) %reduce-scatter.2.cloned.1.call-update) | async-done | bytes 524304 | tf_op jit(solution)/shard_map/reduce_scatter | solution.py:103
  479.2 2.0 add_convert_fusion
  (73 shorter events, 4.8 us)
Async XLA Ops:
  6.5 24.3 %copy-start.7 = (f32[512,128]{1,0:T(8,128)S(1)}, f32[512,128]{1,0:T(8,128)}, u32[]{:S(2)}) copy-start(f32[512,128]{1,0:T(8,128)} %param.22) | copy-start | bytes 786436
  6.5 24.4 %copy-start.9 = (f32[512]{0:T(512)S(1)}, f32[512]{0:T(512)}, u32[]{:S(2)}) copy-start(f32[512]{0:T(512)} %param.28) | copy-start | bytes 6148
  6.5 69.7 %all-gather.8.cloned.1.call-start = ((), (), s32[]{:S(2)}) async-start(), calls=%async_computation.2 | async-start | bytes 2621440 | tf_op jit(solution)/shard_map/all_gather | solution.py:47
  26.3 48.9 %all-to-all-start = ((bf16[128,4,512]{0,2,1:T(8,128)(2,1)}), bf16[128,4,512]{0,2,1:T(8,128)(2,1)S(1)}, u32[]{:S(2)}, u32[]{:S(2)}) async-start(bf16[128,4,512]{0,2,1:T(8,128)(2,1)} %bitcast.7), calls=%async_computation | async-start | bytes 1048576 | tf_op jit(solution)/shard_map/all_to_all | solution.py:82
  29.8 48.6 %copy-start.13 = (f32[2048]{0:T(1024)S(1)}, f32[2048]{0:T(1024)}, u32[]{:S(2)}) copy-start(f32[2048]{0:T(1024)} %param.19) | copy-start | bytes 24580
  29.8 48.6 %copy-start.17 = (f32[128]{0:T(128)S(1)}, f32[128]{0:T(128)}, u32[]{:S(2)}) copy-start(f32[128]{0:T(128)} %param.23) | copy-start | bytes 1540
  29.8 85.2 %all-gather.10.cloned.1.call-start = ((), (), s32[]{:S(2)}) async-start(), calls=%async_computation.3 | async-start | bytes 2621440 | tf_op jit(solution)/shard_map/all_gather | solution.py:88
  78.4 3.0 copy-start.12
  80.9 1.6 copy-start.3
  80.9 1.6 copy-start.18
  82.5 10.3 %copy-start.5 = (bf16[512,512]{1,0:T(8,128)(2,1)S(1)}, bf16[512,512]{1,0:T(8,128)(2,1)}, u32[]{:S(2)}) copy-start(bf16[512,512]{1,0:T(8,128)(2,1)} %param.18) | copy-start | bytes 1572868
  82.5 10.3 %copy-start.6 = (bf16[4,128,512]{2,1,0:T(8,128)(2,1)S(1)}, bf16[4,128,512]{2,1,0:T(8,128)(2,1)}, u32[]{:S(2)}) copy-start(bf16[4,128,512]{2,1,0:T(8,128)(2,1)} %copy.49) | copy-start | bytes 1572868
  84.5 9.7 %copy-start = (f32[512,1408]{1,0:T(8,128)S(1)}, f32[512,1408]{1,0:T(8,128)}, u32[]{:S(2)}) copy-start(f32[512,1408]{1,0:T(8,128)} %param.30) | copy-start | bytes 8650756
  94.1 129.2 %all-gather.12.cloned.1.call-start = ((), (), s32[]{:S(2)}) async-start(), calls=%async_computation.4 | async-start | bytes 7208960 | tf_op jit(solution)/shard_map/all_gather | solution.py:93
  95.5 3.4 copy-start.1
  95.5 234.2 %all-gather.14.cloned.1.call-start = ((), (), s32[]{:S(2)}) async-start(), calls=%async_computation.5 | async-start | bytes 7208960 | tf_op jit(solution)/shard_map/all_gather | solution.py:94
  98.8 1.5 copy-start.10
  98.8 124.5 %copy-start.14 = (f32[1408]{0:T(1024)S(1)}, f32[1408]{0:T(1024)}, u32[]{:S(2)}) copy-start(f32[1408]{0:T(1024)} %param.31) | copy-start | bytes 16900
  98.8 124.5 %copy-start.15 = (f32[2048]{0:T(1024)S(1)}, f32[2048]{0:T(1024)}, u32[]{:S(2)}) copy-start(f32[2048]{0:T(1024)} %param.29) | copy-start | bytes 24580
  98.8 337.3 %all-gather.16.cloned.1.call-start = ((), (), s32[]{:S(2)}) async-start(), calls=%async_computation.6 | async-start | bytes 7208960 | tf_op jit(solution)/shard_map/all_gather | solution.py:101
  100.3 378.9 %reduce-scatter.2.cloned.1.call-start = ((), (), s32[]{:S(2)}) async-start(), calls=%async_computation.7 | async-start | bytes 2621440 | tf_op jit(solution)/shard_map/reduce_scatter | solution.py:103
  117.1 319.0 %copy-start.4 = (bf16[512,2048]{1,0:T(8,128)(2,1)S(1)}, bf16[512,2048]{1,0:T(8,128)(2,1)}, u32[]{:S(2)}) copy-start(bf16[512,2048]{1,0:T(8,128)(2,1)} %all-gather.10.cloned.1.call-done) | copy-start | bytes 6291460
  117.1 319.0 %copy-start.16 = (f32[1408]{0:T(1024)S(1)}, f32[1408]{0:T(1024)}, u32[]{:S(2)}) copy-start(f32[1408]{0:T(1024)} %param.33) | copy-start | bytes 16900
  436.1 43.1 %copy-start.2 = (bf16[512,512]{1,0:T(8,128)(2,1)S(1)}, bf16[512,512]{1,0:T(8,128)(2,1)}, u32[]{:S(2)}) copy-start(bf16[512,512]{1,0:T(8,128)(2,1)} %fusion.11) | copy-start | bytes 1572868
  (2 other events, 1.7 us)
Sparse Core Ops, SparseCore 0:
  8.9 25.2 all-gather.7
  94.2 20.7 all-gather.9
  116.6 106.6 all-gather.11
  224.7 104.9 all-gather.13
  331.1 104.9 all-gather.15
  449.7 29.4 reduce-scatter.1
where the time goes:
time: 488 us
  waiting for transfers between devices  344 us (70%)
  blocking collectives  82.7 us (17%)
  matrix products  27.5 us (6%)
  between operations  13.8 us (3%)
  other arithmetic  13.2 us (3%)
    all_gather x1, waiting for transfers between devices, shards(): lax.all_gather(down_weight.astype(jnp.bfloat16), 'fs', axis=1, tiled=True)  106 us
    all_gather x1, waiting for transfers between devices, shards(): lax.all_gather(gate_cast, 'fs', axis=0, tiled=True)  106 us
    all_gather x1, waiting for transfers between devices, shards(): lax.all_gather(up_cast, 'fs', axis=0, tiled=True)  98.1 us
    reduce_scatter x1, waiting for transfers between devices, shards(): lax.psum_scatter(ffn_terms.astype(jnp.bfloat16), 'tp', scatter_dimension=...  29.6 us
    all_gather x1, blocking collectives, shards(): out_rows = lax.all_gather(out_cast, 'fs', axis=1, tiled=True)  18 us
    all_gather x1, blocking collectives, shards(): lax.all_gather(v_weight.astype(jnp.bfloat16), 'fs', axis=0, tiled=True)  16 us
    all_gather x1, blocking collectives, shards(): lax.all_gather(u_weight.astype(jnp.bfloat16), 'fs', axis=0, tiled=True)  15.9 us
    dot_general x1, matrix products, project_cols(): jnp.dot(source, piece, preferred_element_type=jnp.float32) * scale_whole  13.5 us
  transfers between devices with their start and end apart: 7, of which 5 were waited for; matrix products, arithmetic and copies ran while one was open for 4% of the time, Pallas kernels for 0%

commit v1 on v0

--- a/solution.py
+++ b/solution.py
@@ -20,6 +20,12 @@
 
 def project_cols(source, scale_whole, piece):
     return jnp.dot(source, piece, preferred_element_type=jnp.float32) * scale_whole
+
+
+def gather_shared(piece, axis):
+    width = piece.shape[axis] // lax.axis_size("rep")
+    part = lax.dynamic_slice_in_dim(piece, lax.axis_index("rep") * width, width, axis)
+    return lax.all_gather(part, ("fs", "rep"), axis=axis, tiled=True)
 
 
 def shards(
@@ -90,15 +96,15 @@
     gate_acc, up_acc = fold_pair(
         normed_ffn,
         (
-            lax.all_gather(gate_cast, "fs", axis=0, tiled=True),
-            lax.all_gather(up_cast, "fs", axis=0, tiled=True),
+            gather_shared(gate_cast, 0),
+            gather_shared(up_cast, 0),
         ),
     )
     hidden = (jax.nn.silu(gate_acc * gate_scale) * (up_acc * up_scale)).astype(jnp.bfloat16)
     ffn_terms = project_cols(
         hidden,
         down_whole,
-        lax.all_gather(down_weight.astype(jnp.bfloat16), "fs", axis=1, tiled=True),
+        gather_shared(down_weight.astype(jnp.bfloat16), 1),
     )
     ffn_own = lax.psum_scatter(
         ffn_terms.astype(jnp.bfloat16), "tp", scatter_dimension=1, tiled=True

time: 488 us -> 462 us (0.947)
  waiting for transfers between devices: 344 us -> 304 us
  local copies, waits for them, and re-layouts: 3.48 us -> 15.9 us
    all_gather x3, waiting for transfers between devices: 311 us -> 270 us  [gather_shared(): return lax.all_gather(part, ('fs', 'rep'), axis=axis, tiled=True)]
    convert_element_type x3 -> x0, other arithmetic: 5.9 us -> none  [the longest x1 3.26 us: shards(): up_cast = up_weight.astype(jnp.bfloat16)]
    convert_element_type x0 -> x3, local copies, waits for them, and re-layouts: none -> 5.59 us  [the longest x1 2.31 us: shards(): down_weight.astype(jnp.bfloat16)]
  transfers between devices with their start and end apart: 7 -> 7, of which waited for: 5 -> 5; matrix products, arithmetic and copies ran while one was open for 4% -> 5% of each run, Pallas kernels for 0% -> 0%
where the time goes in v1:
time: 462 us; the launch traced here: 461 us
  waiting for transfers between devices  304 us (66%)
  blocking collectives  83 us (18%)
  matrix products  30.5 us (7%)
  local copies, waits for them, and re-layouts  15.9 us (3%)
  between operations  13.6 us (3%)
  other arithmetic  9.82 us (2%)
    all_gather x3, waiting for transfers between devices, gather_shared(): return lax.all_gather(part, ('fs', 'rep'), axis=axis, tiled=True)  270 us
    reduce_scatter x1, waiting for transfers between devices, shards(): lax.psum_scatter(ffn_terms.astype(jnp.bfloat16), 'tp', scatter_dimension=...  29.5 us
    all_gather x1, blocking collectives, shards(): out_rows = lax.all_gather(out_cast, 'fs', axis=1, tiled=True)  18 us
    all_gather x1, blocking collectives, shards(): lax.all_gather(v_weight.astype(jnp.bfloat16), 'fs', axis=0, tiled=True)  16.9 us
    all_gather x1, blocking collectives, shards(): lax.all_gather(u_weight.astype(jnp.bfloat16), 'fs', axis=0, tiled=True)  15.5 us
    dot_general x1, matrix products, project_cols(): jnp.dot(source, piece, preferred_element_type=jnp.float32) * scale_whole  14.1 us
    all_gather x1, blocking collectives, shards(): lax.all_gather(out_scale, 'fs', axis=0, tiled=True)  12.3 us
    all_gather x1, blocking collectives, shards(): lax.all_gather(down_scale, 'fs', axis=0, tiled=True)  12.1 us
  transfers between devices with their start and end apart: 7, of which 5 were waited for; matrix products, arithmetic and copies ran while one was open for 5% of the time, Pallas kernels for 0%

profile of v1, /device:TPU:0, one launch (start us, length us, event | category | flops | bytes accessed | tf_op | source)
XLA Modules:
  0.0 461.1 jit_solution(16257187439557771775)
XLA Ops:
  8.5 18.0 %all_gather.37 = bf16[128,2048]{0,1:T(8,128)(2,1)} all-gather(bf16[128,512]{0,1:T(8,128)(2,1)S(1)} %copy.48), channel_id=1, replica_groups=mesh['rep'=2,'fs'=4,'tp'=4] {'fs'}, dimensions={1}, use_global_device_ids=true | all-gather | bytes 655360 | tf_op jit(solution)/shard_map/all_gather | solution.py:87
  26.5 3.5 all-to-all-start
  31.0 1.6 convert_element_type.67
  32.6 12.3 %all-gather = f32[4,1,512]{2,1,0:T(1,128)S(1)} all-gather(f32[1,1,512]{2,1,0:T(1,128)S(1)} %bitcast.39), channel_id=1, replica_groups=mesh['rep'=2,'fs'=4,'tp'=4] {'fs'}, dimensions={0}, use_global_device_ids=true | all-gather | bytes 10240 | tf_op jit(solution)/shard_map/all_gather | solution.py:64
  45.6 16.9 %all_gather.35 = bf16[2048,128]{1,0:T(8,128)(2,1)} all-gather(bf16[512,128]{1,0:T(8,128)(2,1)} %convert_element_type.67), channel_id=1, replica_groups=mesh['rep'=2,'fs'=4,'tp'=4] {'fs'}, dimensions={0}, use_global_device_ids=true | all-gather | bytes 655360 | tf_op jit(solution)/shard_map/all_gather | solution.py:60
  62.5 15.5 %all_gather.34 = bf16[2048,128]{1,0:T(8,128)(2,1)} all-gather(bf16[512,128]{1,0:T(8,128)(2,1)S(1)} %convert_element_type.66), channel_id=1, replica_groups=mesh['rep'=2,'fs'=4,'tp'=4] {'fs'}, dimensions={0}, use_global_device_ids=true | all-gather | bytes 655360 | tf_op jit(solution)/shard_map/all_gather | solution.py:59
  79.0 2.1 fusion
  81.7 2.5 fusion.39
  87.0 1.8 copy.42
  90.0 1.8 fusion.12
  94.0 2.6 fusion.30
  96.7 8.1 %all_gather.36 = bf16[512,512]{1,0:T(8,128)(2,1)S(1)} all-gather(bf16[512,128]{1,0:T(8,128)(2,1)S(1)} %fusion.30), channel_id=1, replica_groups=mesh['rep'=2,'fs'=4,'tp'=4] {'tp'}, dimensions={1}, use_global_device_ids=true | all-gather | bytes 655360 | tf_op jit(solution)/shard_map/all_gather | solution.py:86
  107.2 2.3 dynamic-slice_convert_fusion.1
  109.5 2.3 dynamic-slice_convert_fusion
  111.9 12.1 %all-gather.1 = f32[4,1,512]{2,1,0:T(1,128)S(1)} all-gather(f32[1,1,512]{2,1,0:T(1,128)S(1)} %bitcast.40), channel_id=1, replica_groups=mesh['rep'=2,'fs'=4,'tp'=4] {'fs'}, dimensions={0}, use_global_device_ids=true | all-gather | bytes 10240 | tf_op jit(solution)/shard_map/all_gather | solution.py:65
  124.0 4.2 all-gather.10.cloned.1.call-done
  128.3 2.1 fusion.3
  130.4 92.4 %all-gather.12.cloned.1.call-done = bf16[2048,1408]{1,0:T(8,128)(2,1)} async-done(((bf16[256,1408]{1,0:T(8,128)(2,1)}), bf16[2048,1408]{1,0:T(8,128)(2,1)}) %all-gather.12.cloned.1.call-update) | async-done | bytes 5767184 | tf_op jit(solution)/shard_map/all_gather | solution.py:28
  222.8 8.3 %convolution_multiply_fusion.1 = f32[512,1408]{1,0:T(8,128)} fusion(bf16[2048,1408]{1,0:T(8,128)(2,1)} %all-gather.12.cloned.1.call-done, f32[1408]{0:T(1024)S(1)} %copy-done.8, bf16[512,2048]{1,0:T(8,128)(2,1)} %all-gather.10.cloned.1.call-done, f32[2048]{0:T(1024)S(1)} %copy-done.9, f32[512]{0:T(512)S(1)} %add_rsqrt_fusion.1), kind=kOutput, calls=%fused_computation.13 | convolution fusion | flops 2957705216 | bytes 10763776 | tf_op jit(solution)/shard_map/dot_general | solution.py:16
  231.1 84.3 %all-gather.14.cloned.1.call-done = bf16[2048,1408]{1,0:T(8,128)(2,1)} async-done(((bf16[256,1408]{1,0:T(8,128)(2,1)}), bf16[2048,1408]{1,0:T(8,128)(2,1)}) %all-gather.14.cloned.1.call-update) | async-done | bytes 5767184 | tf_op jit(solution)/shard_map/all_gather | solution.py:28
  315.4 93.2 %all-gather.16.cloned.1.call-done = bf16[1408,2048]{1,0:T(8,128)(2,1)} async-done(((bf16[1408,256]{1,0:T(8,128)(2,1)}), bf16[1408,2048]{1,0:T(8,128)(2,1)}) %all-gather.16.cloned.1.call-update) | async-done | bytes 5767184 | tf_op jit(solution)/shard_map/all_gather | solution.py:28
  408.6 14.1 %multiply_convert_fusion = bf16[512,2048]{1,0:T(8,128)(2,1)} fusion(bf16[1408,2048]{1,0:T(8,128)(2,1)} %all-gather.16.cloned.1.call-done, f32[2048]{0:T(1024)S(1)} %bitcast.38, bf16[2048,1408]{1,0:T(8,128)(2,1)} %all-gather.14.cloned.1.call-done, f32[512,1408]{1,0:T(8,128)} %convolution_multiply_fusion.1, f32[1408]{0:T(1024)S(1)} %copy-done.10, ...), kind=kOutput, calls=%fused_computation.10 | convolution fusion | flops 5916917760 | bytes 18636288 | tf_op jit(solution)/shard_map/dot_general | solution.py:22
  422.7 29.5 %reduce-scatter.2.cloned.1.call-done = bf16[512,512]{1,0:T(8,128)(2,1)} async-done(((bf16[512,2048]{1,0:T(8,128)(2,1)}), bf16[512,512]{1,0:T(8,128)(2,1)}) %reduce-scatter.2.cloned.1.call-update) | async-done | bytes 524304 | tf_op jit(solution)/shard_map/reduce_scatter | solution.py:109
  452.3 2.0 add_convert_fusion
  (57 shorter events, 13.8 us)
Async XLA Ops:
  6.5 99.5 %copy-start = (f32[512,1408]{1,0:T(8,128)S(1)}, f32[512,1408]{1,0:T(8,128)}, u32[]{:S(2)}) copy-start(f32[512,1408]{1,0:T(8,128)} %param.30) | copy-start | bytes 8650756
  6.5 26.1 %copy-start.4 = (f32[512]{0:T(512)S(1)}, f32[512]{0:T(512)}, u32[]{:S(2)}) copy-start(f32[512]{0:T(512)} %param.28) | copy-start | bytes 6148
  6.5 72.5 %all-gather.8.cloned.1.call-start = ((), (), s32[]{:S(2)}) async-start(), calls=%async_computation.2 | async-start | bytes 2621440 | tf_op jit(solution)/shard_map/all_gather | solution.py:53
  26.5 51.5 %all-to-all-start = ((bf16[128,4,512]{0,2,1:T(8,128)(2,1)}), bf16[128,4,512]{0,2,1:T(8,128)(2,1)S(1)}, u32[]{:S(2)}, u32[]{:S(2)}) async-start(bf16[128,4,512]{0,2,1:T(8,128)(2,1)} %bitcast.7), calls=%async_computation | async-start | bytes 1048576 | tf_op jit(solution)/shard_map/all_to_all | solution.py:88
  29.9 98.4 %all-gather.10.cloned.1.call-start = ((), (), s32[]{:S(2)}) async-start(), calls=%async_computation.3 | async-start | bytes 2621440 | tf_op jit(solution)/shard_map/all_gather | solution.py:94
  81.1 0.6 copy-start.7
  94.0 10.7 %copy-start.2 = (bf16[512,512]{1,0:T(8,128)(2,1)S(1)}, bf16[512,512]{1,0:T(8,128)(2,1)}, u32[]{:S(2)}) copy-start(bf16[512,512]{1,0:T(8,128)(2,1)} %param.18) | copy-start | bytes 1572868
  94.0 10.7 %copy-start.3 = (bf16[4,128,512]{2,1,0:T(8,128)(2,1)S(1)}, bf16[4,128,512]{2,1,0:T(8,128)(2,1)}, u32[]{:S(2)}) copy-start(bf16[4,128,512]{2,1,0:T(8,128)(2,1)} %copy.49) | copy-start | bytes 1572868
  94.0 10.7 %copy-start.6 = (f32[512]{0:T(512)S(1)}, f32[512]{0:T(512)}, u32[]{:S(2)}) copy-start(f32[512]{0:T(512)} %dynamic_slice.12) | copy-start | bytes 6148
  106.0 116.8 %all-gather.12.cloned.1.call-start = ((), (), s32[]{:S(2)}) async-start(), calls=%async_computation.4 | async-start | bytes 6488064 | tf_op jit(solution)/shard_map/all_gather | solution.py:28
  107.0 4.9 %copy-start.5 = (f32[512]{0:T(512)S(1)}, f32[512]{0:T(512)}, u32[]{:S(2)}) copy-start(f32[512]{0:T(512)} %param.35) | copy-start | bytes 6148
  107.1 115.8 %copy-start.8 = (f32[1408]{0:T(1024)S(1)}, f32[1408]{0:T(1024)}, u32[]{:S(2)}) copy-start(f32[1408]{0:T(1024)} %param.31) | copy-start | bytes 16900
  107.1 115.7 %copy-start.9 = (f32[2048]{0:T(1024)S(1)}, f32[2048]{0:T(1024)}, u32[]{:S(2)}) copy-start(f32[2048]{0:T(1024)} %param.29) | copy-start | bytes 24580
  107.1 208.3 %all-gather.14.cloned.1.call-start = ((), (), s32[]{:S(2)}) async-start(), calls=%async_computation.5 | async-start | bytes 6488064 | tf_op jit(solution)/shard_map/all_gather | solution.py:28
  109.5 299.1 %all-gather.16.cloned.1.call-start = ((), (), s32[]{:S(2)}) async-start(), calls=%async_computation.6 | async-start | bytes 6488064 | tf_op jit(solution)/shard_map/all_gather | solution.py:28
  111.9 340.4 %reduce-scatter.2.cloned.1.call-start = ((), (), s32[]{:S(2)}) async-start(), calls=%async_computation.7 | async-start | bytes 2621440 | tf_op jit(solution)/shard_map/reduce_scatter | solution.py:109
  130.4 278.3 %copy-start.10 = (f32[1408]{0:T(1024)S(1)}, f32[1408]{0:T(1024)}, u32[]{:S(2)}) copy-start(f32[1408]{0:T(1024)} %param.33) | copy-start | bytes 16900
  408.6 43.6 %copy-start.1 = (bf16[512,512]{1,0:T(8,128)(2,1)S(1)}, bf16[512,512]{1,0:T(8,128)(2,1)}, u32[]{:S(2)}) copy-start(bf16[512,512]{1,0:T(8,128)(2,1)} %fusion.11) | copy-start | bytes 1572868
Sparse Core Ops, SparseCore 0:
  8.9 25.2 all-gather.7
  106.1 22.1 all-gather.9
  130.5 92.2 all-gather.11
  224.9 90.4 all-gather.13
  317.3 91.2 all-gather.15
  422.9 29.3 reduce-scatter.1

commit v2 on v0

v2 whole, which is shorter than its diff:
```python
import functools

import jax
import jax.numpy as jnp
from jax import lax
from jax.experimental import pallas as pl
from jax.experimental.pallas import tpu as pltpu
from jax.sharding import PartitionSpec as P

EPS = 0.02
MESH = pl.DeviceIdType.MESH
SCALES, MIXER_IN, MIXER_OUT, GATE, UP, DOWN_A, DOWN_B = range(7)
KINDS = 7
TOKENS, OUT_ROWS, GATED = range(3)


def layer_kernel(
    sizes,
    tokens_ref,
    scales_ref,
    uv_ref,
    out_ref,
    gate_ref,
    up_ref,
    down_ref,
    pre_gain_ref,
    ffn_gain_ref,
    u_scale_ref,
    v_scale_ref,
    group_gain_ref,
    lower_ref,
    bias_ref,
    gate_scale_ref,
    up_scale_ref,
    result_ref,
    tok_all,
    scale_all,
    uv_all,
    out_all,
    gate_all,
    up_all,
    down_all,
    normed,
    gated_all,
    gate_acc,
    up_acc,
    hidden,
    ffn_acc,
    part,
    parts_in,
    local_sem,
    ring_send,
    ring_recv,
    tp_send,
    tp_recv,
    part_send,
    part_recv,
):
    n_rep, n_fs, n_tp = sizes
    n_ring = n_rep * n_fs
    far, near = n_ring // 2, n_ring - 1 - n_ring // 2
    hops = {SCALES: (far, near), MIXER_IN: (far, near), MIXER_OUT: (near, far), GATE: (far, near),
            UP: (near, far), DOWN_A: (far, near), DOWN_B: (near, far)}
    rows, own_width = tokens_ref.shape
    block = normed.shape[2]
    per_own = own_width // block
    rep, fs, tp = lax.axis_index("rep"), lax.axis_index("fs"), lax.axis_index("tp")

    def place(r, f):
        return r * n_fs + jnp.where(lax.rem(r, 2) == 0, f, n_fs - 1 - f)

    def coords(q):
        r, f = q // n_fs, lax.rem(q, n_fs)
        return r, jnp.where(lax.rem(r, 2) == 0, f, n_fs - 1 - f)

    me = place(rep, fs)

    def at_hop(way, hop):
        return lax.rem(me - hop + n_ring, n_ring) if way == 0 else lax.rem(me + hop, n_ring)

    def ring_id(way):
        r, f = coords(at_hop(1 - way, 1))
        return {"rep": r, "fs": f}

    uv_rows, out_rows, down_rows = uv_ref.shape[1], out_ref.shape[0], down_ref.shape[0]
    half = down_rows // 2

    def slot(kind, q):
        r, f = coords(q)
        if kind == SCALES:
            return scale_all.at[q]
        if kind == MIXER_IN:
            return uv_all.at[f, :, pl.ds(pl.multiple_of(r * uv_rows, uv_rows), uv_rows)]
        if kind == MIXER_OUT:
            return out_all.at[f, tp, pl.ds(pl.multiple_of(r * out_rows, out_rows), out_rows)]
        if kind == GATE:
            return gate_all.at[q]
        if kind == UP:
            return up_all.at[q]
        return down_all.at[q, pl.ds(0 if kind == DOWN_A else half, half)]

    def send(kind, way, hop):
        ref = slot(kind, at_hop(way, hop - 1))
        return pltpu.make_async_remote_copy(
            src_ref=ref, dst_ref=ref, send_sem=ring_send.at[kind, way, hop - 1],
            recv_sem=ring_recv.at[kind, way, hop - 1], device_id=ring_id(way), device_id_type=MESH)

    def wait_hop(kind, way, hop):
        ref = slot(kind, at_hop(way, hop))
        pltpu.make_async_remote_copy(
            src_ref=ref, dst_ref=ref, send_sem=ring_send.at[kind, way, hop - 1],
            recv_sem=ring_recv.at[kind, way, hop - 1], device_id=ring_id(way),
            device_id_type=MESH).wait_recv()

    def on(condition, action):
        if isinstance(condition, bool):
            if condition:
                action()
        else:
            pl.when(condition)(action)

    def begin(kind):
        for way in range(2):
            send(kind, way, 1).start()

    def pump(kind, hop):
        for way in range(2):
            def take(way=way):
                wait_hop(kind, way, hop)
                on(hop < hops[kind][way], lambda: send(kind, way, hop + 1).start())
            on(hop <= hops[kind][way], take)

    def tp_ref(kind, t):
        if kind == TOKENS:
            return tok_all.at[t]
        if kind == OUT_ROWS:
            return out_all.at[:, t]
        return gated_all.at[t]

    def tp_copy(kind, k, t):
        ref = tp_ref(kind, t)
        return pltpu.make_async_remote_copy(
            src_ref=ref, dst_ref=ref, send_sem=tp_send.at[kind, k - 1],
            recv_sem=tp_recv.at[kind, k - 1], device_id={"tp": lax.rem(tp + k, n_tp)},
            device_id_type=MESH)

    def tp_start(kind):
        for k in range(1, n_tp):
            tp_copy(kind, k, tp).start()

    def tp_wait(kind):
        for k in range(1, n_tp):
            tp_copy(kind, k, lax.rem(tp - k + n_tp, n_tp)).wait_recv()

    own = [
        pltpu.make_async_copy(tokens_ref, tok_all.at[tp], local_sem.at[0]),
        pltpu.make_async_copy(scales_ref, slot(SCALES, me), local_sem.at[1]),
        pltpu.make_async_copy(uv_ref, slot(MIXER_IN, me), local_sem.at[2]),
        pltpu.make_async_copy(out_ref, slot(MIXER_OUT, me), local_sem.at[3]),
        pltpu.make_async_copy(gate_ref, gate_all.at[me], local_sem.at[4]),
        pltpu.make_async_copy(up_ref, up_all.at[me], local_sem.at[5]),
        pltpu.make_async_copy(down_ref, down_all.at[me], local_sem.at[6]),
    ]
    for copy in own:
        copy.start()
    barrier = pltpu.get_barrier_semaphore()
    for way in range(2):
        pl.semaphore_signal(barrier, inc=1, device_id=ring_id(way), device_id_type=MESH)
    for k in range(1, n_tp):
        pl.semaphore_signal(barrier, inc=1, device_id={"tp": lax.rem(tp + k, n_tp)},
                            device_id_type=MESH)
    pl.semaphore_wait(barrier, 2 + n_tp - 1)
    for copy in own:
        copy.wait()

    tp_start(TOKENS)
    for kind in (MIXER_IN, MIXER_OUT, SCALES):
        begin(kind)

    def small_step(hop, carry):
        for kind in (MIXER_IN, MIXER_OUT, SCALES):
            pump(kind, hop)
        return carry

    lax.fori_loop(1, far, small_step, 0)
    begin(GATE)
    begin(UP)
    small_step(far, 0)
    tp_start(OUT_ROWS)
    tp_wait(TOKENS)

    span = lower_ref.shape[1]
    groups = lower_ref.shape[0]

    def span_rows(i):
        return pl.ds(pl.multiple_of(i * span, span), span)

    def norm_span(i, gain_ref):
        here = span_rows(i)
        square = jnp.zeros((span, 1), jnp.float32)
        for t in range(n_tp):
            wide = tok_all[t, here, :].astype(jnp.float32)
            square += jnp.sum(wide * wide, axis=-1, keepdims=True)
        inverse = lax.rsqrt(square / (n_tp * own_width) + EPS)
        for f in range(n_fs):
            t, sub = f // per_own, f % per_own
            wide = tok_all[t, here, sub * block:(sub + 1) * block].astype(jnp.float32)
            gain = gain_ref[:, f * block:(f + 1) * block]
            normed[f, here, :] = (wide * inverse * gain).astype(jnp.bfloat16)

    def mixer_span(i, carry):
        here = span_rows(i)
        norm_span(i, pre_gain_ref)
        u_pre = v_pre = None
        for f in range(n_fs):
            source = normed[f, here, :]
            u_term = jnp.dot(source, uv_all[f, 0], preferred_element_type=jnp.float32)
            v_term = jnp.dot(source, uv_all[f, 1], preferred_element_type=jnp.float32)
            u_pre = u_term if f == 0 else u_pre + u_term
            v_pre = v_term if f == 0 else v_pre + v_term
        u_act = jax.nn.gelu(u_pre * u_scale_ref[...])
        v_act = jax.nn.gelu(v_pre * v_scale_ref[...])
        width = v_act.shape[1] // groups
        group_of = lax.broadcasted_iota(jnp.int32, v_act.shape, 1) // width
        centre = jnp.zeros_like(v_act)
        for g in range(groups):
            mean = jnp.sum(jnp.where(group_of == g, v_act, 0.0), axis=-1, keepdims=True) / width
            centre = jnp.where(group_of == g, mean, centre)
        apart = v_act - centre
        square = apart * apart
        inverse = jnp.zeros_like(v_act)
        for g in range(groups):
            spread = jnp.sum(jnp.where(group_of == g, square, 0.0), axis=-1, keepdims=True) / width
            inverse = jnp.where(group_of == g, lax.rsqrt(spread + EPS), inverse)
        v_norm = (apart * inverse * group_gain_ref[...]).astype(jnp.bfloat16)
        mixed = bias_ref[...]
        for g in range(groups):
            term = jnp.dot(lower_ref[g], v_norm, preferred_element_type=jnp.float32)
            mixed = mixed + jnp.where(group_of == g, term, 0.0)
        gated_all[tp, here, :] = (u_act * mixed).astype(jnp.bfloat16)
        return carry

    spans = rows // span
    lax.fori_loop(0, spans, mixer_span, 0)
    tp_start(GATED)
    pump(GATE, 1)
    tp_wait(OUT_ROWS)
    tp_wait(GATED)

    def resid_span(i, carry):
        here = span_rows(i)
        for f in range(n_fs):
            t, sub = f // per_own, f % per_own
            mix = None
            for s in range(n_tp):
                term = jnp.dot(gated_all[s, here, :], out_all[f, s],
                               preferred_element_type=jnp.float32)
                mix = term if s == 0 else mix + term
            mix = (mix * scale_all[f, 0:1, :]).astype(jnp.bfloat16)
            cols = slice(sub * block, (sub + 1) * block)
            tok_all[t, here, cols] = (
                tok_all[t, here, cols].astype(jnp.float32) + mix.astype(jnp.float32)
            ).astype(jnp.bfloat16)
        norm_span(i, ffn_gain_ref)
        return carry

    for k in range(1, n_tp):
        tp_copy(TOKENS, k, tp).wait_send()
    lax.fori_loop(0, spans, resid_span, 0)
    pump(UP, 1)

    chunk = span
    chunks = rows // chunk

    def fold(acc, weights, q):
        r, f = coords(q)

        def body(i, carry):
            here = pl.ds(pl.multiple_of(i * chunk, chunk), chunk)
            term = jnp.dot(normed[f, here, :], weights[q], preferred_element_type=jnp.float32)
            acc[r, here, :] = acc[r, here, :] + term
            return carry

        lax.fori_loop(0, chunks, body, 0)

    gate_acc[...] = jnp.zeros_like(gate_acc)
    up_acc[...] = jnp.zeros_like(up_acc)
    fold(gate_acc, gate_all, me)
    fold(up_acc, up_all, me)

    def fold_hop(acc, weights, kind, hop):
        for way in range(2):
            on(hop <= hops[kind][way],
               lambda way=way: fold(acc, weights, at_hop(way, hop)))

    def ffn_step(hop, carry):
        on(hop > 1, lambda: pump(GATE, hop))
        fold_hop(gate_acc, gate_all, GATE, hop)
        on(hop > 1, lambda: pump(UP, hop))

        def start_down():
            begin(DOWN_A)
            begin(DOWN_B)

        on(hop == far - 1, start_down)
        fold_hop(up_acc, up_all, UP, hop)
        return carry

    lax.fori_loop(1, far + 1, ffn_step, 0)

    def hidden_chunk(i, carry):
        here = pl.ds(pl.multiple_of(i * chunk, chunk), chunk)
        for r in range(n_rep):
            a = gate_acc[r, here, :] * gate_scale_ref[r:r + 1, :]
            b = up_acc[r, here, :] * up_scale_ref[r:r + 1, :]
            hidden[r, here, :] = (a / (1.0 + jnp.exp(-a)) * b).astype(jnp.bfloat16)
        return carry

    lax.fori_loop(0, chunks, hidden_chunk, 0)
    ffn_acc[...] = jnp.zeros_like(ffn_acc)

    def fold_down(q, low, size):
        r, f = coords(q)

        def body(i, carry):
            here = pl.ds(pl.multiple_of(i * chunk, chunk), chunk)
            term = jnp.dot(hidden[r, here, :], down_all[q], preferred_element_type=jnp.float32)
            ffn_acc[f, here, :] = ffn_acc[f, here, :] + term
            return carry

        lax.fori_loop(0, chunks, body, 0)

    def part_copy(f, owner, sender):
        sub = lax.rem(f, per_own)
        return pltpu.make_async_remote_copy(
            src_ref=part.at[f], dst_ref=parts_in.at[sender, sub], send_sem=part_send.at[f],
            recv_sem=part_recv.at[sender, sub], device_id={"tp": owner}, device_id_type=MESH)

    def finish(f):
        def body(i, carry):
            here = pl.ds(pl.multiple_of(i * chunk, chunk), chunk)
            part[f, here, :] = (ffn_acc[f, here, :] * scale_all[f, 1:2, :]).astype(jnp.bfloat16)
            return carry

        lax.fori_loop(0, chunks, body, 0)
        owner = f // per_own
        on(owner != tp, lambda: part_copy(f, owner, tp).start())

    def complete_at(f):
        last = 0
        for r in range(n_rep):
            gap = lax.rem(me - place(r, f) + n_ring, n_ring)
            last = jnp.maximum(last, jnp.minimum(gap, n_ring - gap))
        return last

    fold_down(me, 0, down_rows)

    def down_step(hop, carry):
        pump(DOWN_A, hop)
        pump(DOWN_B, hop)
        fold_down(at_hop(0, hop), 0, down_rows)
        on(hop <= near, lambda: fold_down(at_hop(1, hop), 0, down_rows))

        def finish_if(f, inner):
            on(complete_at(f) == hop, lambda: finish(f))
            return inner

        lax.fori_loop(0, n_fs, finish_if, 0)
        return carry

    lax.fori_loop(1, far + 1, down_step, 0)

    for k in range(1, n_tp):
        sender = lax.rem(tp + k, n_tp)
        for sub in range(per_own):
            part_copy(tp * per_own + sub, tp, sender).wait_recv()

    def close_span(i, carry):
        here = pl.ds(pl.multiple_of(i * chunk, chunk), chunk)
        for sub in range(per_own):
            cols = slice(sub * block, (sub + 1) * block)
            total = part[tp * per_own + sub, here, :].astype(jnp.float32)
            for k in range(1, n_tp):
                total += parts_in[lax.rem(tp + k, n_tp), sub, here, :].astype(jnp.float32)
            total = total.astype(jnp.bfloat16).astype(jnp.float32)
            kept = tok_all[tp, here, cols].astype(jnp.float32)
            result_ref[here, cols] = (kept + total).astype(jnp.bfloat16)
        return carry

    lax.fori_loop(0, chunks, close_span, 0)

    for kind in range(KINDS):
        for way in range(2):
            def sent(hop, carry, kind=kind, way=way):
                send(kind, way, hop).wait_send()
                return carry

            lax.fori_loop(1, hops[kind][way] + 1, sent, 0)
    for kind in (OUT_ROWS, GATED):
        for k in range(1, n_tp):
            tp_copy(kind, k, tp).wait_send()

    def part_sent(f, carry):
        owner = f // per_own
        on(owner != tp, lambda: part_copy(f, owner, tp).wait_send())
        return carry

    lax.fori_loop(0, n_fs, part_sent, 0)


def shards(
    sizes,
    tokens,
    pre_gain,
    u_weight,
    u_scale,
    v_weight,
    v_scale,
    group_gain,
    span_weight,
    span_bias,
    out_weight,
    out_scale,
    ffn_gain,
    gate_weight,
    gate_scale,
    up_weight,
    up_scale,
    down_weight,
    down_scale,
):
    n_rep, n_fs, n_tp = sizes
    n_ring = n_rep * n_fs
    rep = lax.axis_index("rep")

    def share(array, axis):
        width = array.shape[axis] // n_rep
        return lax.dynamic_slice_in_dim(array, rep * width, width, axis).astype(jnp.bfloat16)

    rows, own_width = tokens.shape
    block, local_hidden = gate_weight.shape
    hid = local_hidden // n_rep
    channels = u_weight.shape[1]
    groups, span = span_weight.shape[0], span_weight.shape[1]
    uv = share(jnp.stack([u_weight, v_weight]), 1)
    scales = jnp.stack([out_scale, down_scale])
    bias = jnp.repeat(jnp.transpose(span_bias), channels // groups, axis=1)
    row = lambda vector: vector.reshape(1, -1)
    operands = (
        tokens, scales, uv, share(out_weight, 0), share(gate_weight, 1), share(up_weight, 1),
        share(down_weight, 0), row(pre_gain), row(ffn_gain), row(u_scale), row(v_scale),
        row(group_gain), jnp.tril(span_weight), bias, gate_scale.reshape(n_rep, hid),
        up_scale.reshape(n_rep, hid),
    )
    hbm, vmem = pl.BlockSpec(memory_space=pl.ANY), pl.BlockSpec(memory_space=pltpu.VMEM)
    bf16, f32 = jnp.bfloat16, jnp.float32
    per_own = own_width // block
    steps = n_ring // 2
    return pl.pallas_call(
        functools.partial(layer_kernel, sizes),
        out_shape=jax.ShapeDtypeStruct((rows, own_width), bf16),
        in_specs=[hbm] * 7 + [vmem] * 9,
        out_specs=vmem,
        scratch_shapes=[
            pltpu.VMEM((n_tp, rows, own_width), bf16),
            pltpu.VMEM((n_ring, 2, block), f32),
            pltpu.VMEM((n_fs, 2, block, channels), bf16),
            pltpu.VMEM((n_fs, n_tp, channels, block), bf16),
            pltpu.VMEM((n_ring, block, hid), bf16),
            pltpu.VMEM((n_ring, block, hid), bf16),
            pltpu.VMEM((n_ring, hid, block), bf16),
            pltpu.VMEM((n_fs, rows, block), bf16),
            pltpu.VMEM((n_tp, rows, channels), bf16),
            pltpu.VMEM((n_rep, rows, hid), f32),
            pltpu.VMEM((n_rep, rows, hid), f32),
            pltpu.VMEM((n_rep, rows, hid), bf16),
            pltpu.VMEM((n_fs, rows, block), f32),
            pltpu.VMEM((n_fs, rows, block), bf16),
            pltpu.VMEM((n_tp, per_own, rows, block), bf16),
            pltpu.SemaphoreType.DMA((7,)),
            pltpu.SemaphoreType.DMA((KINDS, 2, steps)),
            pltpu.SemaphoreType.DMA((KINDS, 2, steps)),
            pltpu.SemaphoreType.DMA((3, n_tp - 1)),
            pltpu.SemaphoreType.DMA((3, n_tp - 1)),
            pltpu.SemaphoreType.DMA((n_fs,)),
            pltpu.SemaphoreType.DMA((n_tp, per_own)),
        ],
        compiler_params=pltpu.CompilerParams(
            collective_id=0, has_side_effects=True, vmem_limit_bytes=62 * 1024 * 1024
        ),
    )(*operands)


def solution(mesh):
    placed = (
        P(("rep", "fs"), "tp"),
        P(),
        P("fs", "tp"),
        P("tp"),
        P("fs", "tp"),
        P("tp"),
        P("tp"),
        P("tp", None, None),
        P("tp", None),
        P("tp", "fs"),
        P("fs"),
        P(),
        P("fs", "tp"),
        P("tp"),
        P("fs", "tp"),
        P("tp"),
        P("tp", "fs"),
        P("fs"),
    )
    sizes = (mesh.shape["rep"], mesh.shape["fs"], mesh.shape["tp"])
    return jax.shard_map(
        functools.partial(shards, sizes), mesh=mesh, in_specs=placed, out_specs=P(("rep", "fs"), "tp"), check_vma=False
    )
```

time: 488 us -> 230 us (0.47)
  waiting for transfers between devices: 344 us -> 0 us
  Pallas kernels: 0 us -> 212 us
  blocking collectives: 82.7 us -> 0 us
  matrix products: 27.5 us -> 0 us
  between operations: 13.8 us -> 0.02 us
  local copies, waits for them, and re-layouts: 3.48 us -> 12.7 us
  other arithmetic: 13.2 us -> 4.46 us
    all_gather x5 -> x0, waiting for transfers between devices: 313 us -> none  [the longest x1 106 us: shards(): lax.all_gather(down_weight.astype(jnp.bfloat16), 'fs', axis=1, tiled=True)]
    pallas_call x0 -> x1, Pallas kernels: none -> 212 us  [shards(): pl.pallas_call(functools.partial(layer_kernel, sizes), out_shape=jax.Shap...]
    all_gather x6 -> x0, blocking collectives: 82.7 us -> none  [the longest x1 18 us: shards(): out_rows = lax.all_gather(out_cast, 'fs', axis=1, tiled=True)]
    reduce_scatter x1 -> x0, waiting for transfers between devices: 29.6 us -> none  [shards(): lax.psum_scatter(ffn_terms.astype(jnp.bfloat16), 'tp', scatter_dimension=...]
    dot_general x6 -> x0, matrix products: 27.5 us -> none  [the longest x1 13.5 us: project_cols(): jnp.dot(source, piece, preferred_element_type=jnp.float32) * scale_whole]
    convert_element_type x7 -> x1, other arithmetic: 8.89 us -> 1.64 us  [share(): lax.dynamic_slice_in_dim(array, rep * width, width, axis)]
    convert_element_type x0 -> x3, local copies, waits for them, and re-layouts: none -> 6.65 us  [share(): lax.dynamic_slice_in_dim(array, rep * width, width, axis)]
  transfers between devices with their start and end apart: 7 -> 0, of which waited for: 5 -> 0; matrix products, arithmetic and copies ran while one was open for 4% -> 0% of each run, Pallas kernels for 0% -> 0%
where the time goes in v2:
time: 230 us; the launch traced here: 229 us
  Pallas kernels  212 us (92%)
  local copies, waits for them, and re-layouts  12.7 us (6%)
  other arithmetic  4.46 us (2%)
    pallas_call x1, Pallas kernels, shards(): pl.pallas_call(functools.partial(layer_kernel, sizes), out_shape=jax.Shap...  212 us
    convert_element_type x3, local copies, waits for them, and re-layouts, share(): lax.dynamic_slice_in_dim(array, rep * width, width, axis)  6.65 us

profile of v2, /device:TPU:0, one launch (start us, length us, event | category | flops | bytes accessed | tf_op | source)
XLA Modules:
  0.0 229.0 jit_solution(5766268063579390711)
XLA Ops:
  0.0 0.0 copy-start
  0.0 1.3 pad_maximum_fusion.scales_ref
  1.3 1.4 reshape.30.gate_scale_ref
  2.7 1.4 reshape.31.up_scale_ref
  4.1 1.5 broadcast_select_fusion.lower_ref
  5.6 0.0 copy-done
  5.6 0.6 dynamic-slice_convert_fusion.3.out_ref
  6.2 0.7 broadcast_in_dim.13
  6.9 0.7 copy.20.bias_ref
  7.6 1.6 fusion.1.uv_ref
  9.2 2.3 %dynamic-slice_convert_fusion.2.down_ref = bf16[704,512]{1,0:T(8,128)(2,1)} fusion(f32[1408,512]{1,0:T(8,128)} %param.34, s32[]{:T(128)S(6)} %select_n.17), kind=kLoop, calls=%fused_computation.2 | loop fusion | bytes 1441796 | tf_op jit(solution)/shard_map/convert_element_type | solution.py:438
  11.5 3.7 %dynamic-slice_convert_fusion = (bf16[512,704]{1,0:T(8,128)(2,1)}, bf16[512,704]{1,0:T(8,128)(2,1)}) fusion(f32[512,1408]{1,0:T(8,128)} %param.32, s32[]{:T(128)S(6)} %select_n.17, f32[512,1408]{1,0:T(8,128)} %param.30), kind=kLoop, calls=%fused_computation | loop fusion | bytes 2883588 | tf_op jit(solution)/shard_map/convert_element_type | solution.py:438
  15.3 211.9 %shard_map.172 = bf16[512,512]{1,0:T(8,128)(2,1)} custom-call(bf16[512,512]{1,0:T(8,128)(2,1)} %tokens_ref.1, f32[2,512]{1,0:T(2,128)} %pad_maximum_fusion.scales_ref, bf16[2,256,128]{2,1,0:T(8,128)(2,1)} %fusion.1.uv_ref, bf16[64,512]{1,0:T(8,128)(2,1)} %dynamic-slice_convert_fusion.3.out_ref, bf16[512,704]{1,0:T(8,128)(2,1)} %get-tuple-element.6.gate_ref, ...), custom_call_target="tpu_custom_call" | custom-call | tf_op jit(solution)/shard_map/pallas_call | solution.py:459
  227.2 1.9 copy.22
  (1 shorter events, 0.0 us)
Async XLA Ops:
  0.0 5.6 %copy-start = (f32[128,512]{1,0:T(8,128)S(1)}, f32[128,512]{1,0:T(8,128)}, u32[]{:S(2)}) copy-start(f32[128,512]{1,0:T(8,128)} %param.27) | copy-start | bytes 786436

commit v3 on v2

v3 whole, which is shorter than its diff:
```python
import functools

import jax
import jax.numpy as jnp
from jax import lax
from jax.experimental import pallas as pl
from jax.experimental.pallas import tpu as pltpu
from jax.sharding import PartitionSpec as P

EPS = 0.02
MESH = pl.DeviceIdType.MESH
SCALES, MIXER_IN, MIXER_OUT, GATE, UP, DOWN_A, DOWN_B = range(7)
KINDS = 7
TOKENS, OUT_ROWS, GATED = range(3)


def layer_kernel(
    sizes,
    tokens_ref,
    out_scale_ref,
    down_scale_ref,
    uv_ref,
    out_ref,
    gate_ref,
    up_ref,
    down_ref,
    pre_gain_ref,
    ffn_gain_ref,
    u_scale_ref,
    v_scale_ref,
    group_gain_ref,
    lower_ref,
    bias_ref,
    gate_scale_ref,
    up_scale_ref,
    result_ref,
    tok_all,
    scale_all,
    uv_all,
    out_all,
    gate_all,
    up_all,
    down_all,
    normed,
    gated_all,
    gate_acc,
    up_acc,
    hidden,
    ffn_acc,
    part,
    parts_in,
    local_sem,
    line_send,
    line_recv,
    rep_send,
    rep_recv,
    tp_send,
    tp_recv,
    part_send,
    part_recv,
):
    n_rep, n_fs, n_tp = sizes
    rows, own_width = tokens_ref.shape
    block = normed.shape[2]
    per_own = own_width // block
    rep, fs, tp = lax.axis_index("rep"), lax.axis_index("fs"), lax.axis_index("tp")

    last_hop = n_fs - 1

    def at_hop(way, hop):
        return fs - hop if way == 0 else fs + hop

    def arrives(way, hop):
        f = at_hop(way, hop)
        return jnp.logical_and(f >= 0, f < n_fs)

    def leaves(way, hop):
        ahead = fs + 1 if way == 0 else fs - 1
        return jnp.logical_and(arrives(way, hop - 1), jnp.logical_and(ahead >= 0, ahead < n_fs))

    uv_rows, out_rows, down_rows = uv_ref.shape[2], out_ref.shape[1], down_ref.shape[1]
    half = down_rows // 2

    def slot(kind, r, f):
        if kind == SCALES:
            return scale_all.at[f]
        if kind == MIXER_IN:
            return uv_all.at[f, :, pl.ds(pl.multiple_of(r * uv_rows, uv_rows), uv_rows)]
        if kind == MIXER_OUT:
            return out_all.at[f, tp, pl.ds(pl.multiple_of(r * out_rows, out_rows), out_rows)]
        if kind == GATE:
            return gate_all.at[r, f]
        if kind == UP:
            return up_all.at[r, f]
        return down_all.at[r, f, pl.ds(0 if kind == DOWN_A else half, half)]

    def line_copy(kind, way, hop, f):
        ref = slot(kind, rep, f)
        return pltpu.make_async_remote_copy(
            src_ref=ref, dst_ref=ref, send_sem=line_send.at[kind, way, hop - 1],
            recv_sem=line_recv.at[kind, way, hop - 1],
            device_id={"fs": fs + 1 if way == 0 else fs - 1}, device_id_type=MESH)

    def send(kind, way, hop):
        return line_copy(kind, way, hop, at_hop(way, hop - 1))

    def rep_copy(kind, way, hop, k, r):
        ref = slot(kind, r, at_hop(way, hop))
        return pltpu.make_async_remote_copy(
            src_ref=ref, dst_ref=ref, send_sem=rep_send.at[kind, way, hop - 1, k - 1],
            recv_sem=rep_recv.at[kind, way, hop - 1, k - 1],
            device_id={"rep": lax.rem(rep + k, n_rep)}, device_id_type=MESH)

    def on(condition, action):
        if isinstance(condition, bool):
            if condition:
                action()
        else:
            pl.when(condition)(action)

    def begin(kind):
        for way in range(2):
            on(leaves(way, 1), lambda way=way: send(kind, way, 1).start())

    def pump(kind, hop):
        for way in range(2):
            def take(way=way):
                line_copy(kind, way, hop, at_hop(way, hop)).wait_recv()
                on(leaves(way, hop + 1), lambda: send(kind, way, hop + 1).start())
                if kind != SCALES:
                    for k in range(1, n_rep):
                        rep_copy(kind, way, hop, k, rep).start()
            on(arrives(way, hop), take)

    def rep_wait(kind, hop):
        for way in range(2):
            def take(way=way):
                for k in range(1, n_rep):
                    rep_copy(kind, way, hop, k, lax.rem(rep - k + n_rep, n_rep)).wait_recv()
            on(arrives(way, hop), take)

    def tp_ref(kind, t):
        if kind == TOKENS:
            return tok_all.at[t]
        if kind == OUT_ROWS:
            return out_all.at[:, t]
        return gated_all.at[t]

    def tp_copy(kind, k, t):
        ref = tp_ref(kind, t)
        return pltpu.make_async_remote_copy(
            src_ref=ref, dst_ref=ref, send_sem=tp_send.at[kind, k - 1],
            recv_sem=tp_recv.at[kind, k - 1], device_id={"tp": lax.rem(tp + k, n_tp)},
            device_id_type=MESH)

    def tp_start(kind):
        for k in range(1, n_tp):
            tp_copy(kind, k, tp).start()

    def tp_wait(kind):
        for k in range(1, n_tp):
            tp_copy(kind, k, lax.rem(tp - k + n_tp, n_tp)).wait_recv()

    own = [
        pltpu.make_async_copy(tokens_ref, tok_all.at[tp], local_sem.at[0]),
        pltpu.make_async_copy(out_scale_ref, scale_all.at[fs, 0], local_sem.at[1]),
        pltpu.make_async_copy(down_scale_ref, scale_all.at[fs, 1], local_sem.at[2]),
    ]
    pairs = [(MIXER_IN, lambda r: uv_ref.at[r]), (MIXER_OUT, lambda r: out_ref.at[r]),
             (GATE, lambda r: gate_ref.at[r]), (UP, lambda r: up_ref.at[r]),
             (DOWN_A, lambda r: down_ref.at[r, pl.ds(0, half)]),
             (DOWN_B, lambda r: down_ref.at[r, pl.ds(half, half)])]
    for i, (kind, source) in enumerate(pairs):
        for r in range(n_rep):
            own.append(pltpu.make_async_copy(
                source(r), slot(kind, r, fs), local_sem.at[3 + i * n_rep + r]))
    for copy in own:
        copy.start()
    barrier = pltpu.get_barrier_semaphore()
    for way in range(2):
        def greet(way=way):
            pl.semaphore_signal(barrier, inc=1, device_id={"fs": fs + 1 if way == 0 else fs - 1},
                                device_id_type=MESH)
        on(leaves(way, 1), greet)
    for k in range(1, n_rep):
        pl.semaphore_signal(barrier, inc=1, device_id={"rep": lax.rem(rep + k, n_rep)},
                            device_id_type=MESH)
    for k in range(1, n_tp):
        pl.semaphore_signal(barrier, inc=1, device_id={"tp": lax.rem(tp + k, n_tp)},
                            device_id_type=MESH)
    beside = (fs > 0).astype(jnp.int32) + (fs < n_fs - 1).astype(jnp.int32)
    pl.semaphore_wait(barrier, beside + n_rep - 1 + n_tp - 1)
    for copy in own:
        copy.wait()

    tp_start(TOKENS)
    small = (MIXER_IN, MIXER_OUT, SCALES)
    for kind in small:
        begin(kind)
    begin(GATE)

    def small_step(hop, carry):
        for kind in small:
            pump(kind, hop)
        return carry

    small_step(1, 0)
    begin(UP)
    small_step(2, 0)
    pump(GATE, 1)
    lax.fori_loop(3, last_hop + 1, small_step, 0)

    def small_rep(hop, carry):
        for kind in (MIXER_IN, MIXER_OUT):
            rep_wait(kind, hop)
        return carry

    lax.fori_loop(1, last_hop + 1, small_rep, 0)
    tp_start(OUT_ROWS)
    tp_wait(TOKENS)

    span = lower_ref.shape[1]
    groups = lower_ref.shape[0]

    def span_rows(i):
        return pl.ds(pl.multiple_of(i * span, span), span)

    def norm_span(i, gain_ref):
        here = span_rows(i)
        square = jnp.zeros((span, 1), jnp.float32)
        for t in range(n_tp):
            wide = tok_all[t, here, :].astype(jnp.float32)
            square += jnp.sum(wide * wide, axis=-1, keepdims=True)
        inverse = lax.rsqrt(square / (n_tp * own_width) + EPS)
        for f in range(n_fs):
            t, sub = f // per_own, f % per_own
            wide = tok_all[t, here, sub * block:(sub + 1) * block].astype(jnp.float32)
            gain = gain_ref[:, f * block:(f + 1) * block]
            normed[f, here, :] = (wide * inverse * gain).astype(jnp.bfloat16)

    def lower_part(g):
        square = lower_ref[g].astype(jnp.float32)
        t = lax.broadcasted_iota(jnp.int32, square.shape, 0)
        s = lax.broadcasted_iota(jnp.int32, square.shape, 1)
        return jnp.where(s <= t, square, 0.0).astype(jnp.bfloat16)

    def mixer_span(i, carry):
        here = span_rows(i)
        norm_span(i, pre_gain_ref)
        u_pre = v_pre = None
        for f in range(n_fs):
            source = normed[f, here, :]
            u_term = jnp.dot(source, uv_all[f, 0], preferred_element_type=jnp.float32)
            v_term = jnp.dot(source, uv_all[f, 1], preferred_element_type=jnp.float32)
            u_pre = u_term if f == 0 else u_pre + u_term
            v_pre = v_term if f == 0 else v_pre + v_term
        u_act = jax.nn.gelu(u_pre * u_scale_ref[...])
        v_act = jax.nn.gelu(v_pre * v_scale_ref[...])
        width = v_act.shape[1] // groups
        group_of = lax.broadcasted_iota(jnp.int32, v_act.shape, 1) // width
        centre = jnp.zeros_like(v_act)
        for g in range(groups):
            mean = jnp.sum(jnp.where(group_of == g, v_act, 0.0), axis=-1, keepdims=True) / width
            centre = jnp.where(group_of == g, mean, centre)
        apart = v_act - centre
        square = apart * apart
        inverse = jnp.zeros_like(v_act)
        for g in range(groups):
            spread = jnp.sum(jnp.where(group_of == g, square, 0.0), axis=-1, keepdims=True) / width
            inverse = jnp.where(group_of == g, lax.rsqrt(spread + EPS), inverse)
        v_norm = (apart * inverse * group_gain_ref[...]).astype(jnp.bfloat16)
        mixed = bias_ref[...]
        for g in range(groups):
            term = jnp.dot(lower_part(g), v_norm, preferred_element_type=jnp.float32)
            mixed = mixed + jnp.where(group_of == g, term, 0.0)
        gated_all[tp, here, :] = (u_act * mixed).astype(jnp.bfloat16)
        return carry

    spans = rows // span
    lax.fori_loop(0, spans, mixer_span, 0)
    tp_start(GATED)
    pump(UP, 1)
    tp_wait(OUT_ROWS)
    tp_wait(GATED)

    def resid_span(i, carry):
        here = span_rows(i)
        for f in range(n_fs):
            t, sub = f // per_own, f % per_own
            mix = None
            for s in range(n_tp):
                term = jnp.dot(gated_all[s, here, :], out_all[f, s],
                               preferred_element_type=jnp.float32)
                mix = term if s == 0 else mix + term
            mix = (mix * scale_all[f, 0]).astype(jnp.bfloat16)
            cols = slice(sub * block, (sub + 1) * block)
            tok_all[t, here, cols] = (
                tok_all[t, here, cols].astype(jnp.float32) + mix.astype(jnp.float32)
            ).astype(jnp.bfloat16)
        norm_span(i, ffn_gain_ref)
        return carry

    for k in range(1, n_tp):
        tp_copy(TOKENS, k, tp).wait_send()
    lax.fori_loop(0, spans, resid_span, 0)

    chunk = span
    chunks = rows // chunk

    def fold(acc, weights, r, f):
        def body(i, carry):
            here = pl.ds(pl.multiple_of(i * chunk, chunk), chunk)
            term = jnp.dot(normed[f, here, :], weights[r, f], preferred_element_type=jnp.float32)
            acc[r, here, :] = acc[r, here, :] + term
            return carry

        lax.fori_loop(0, chunks, body, 0)

    def others():
        return [lax.rem(rep + k, n_rep) for k in range(1, n_rep)]

    def fold_hop(acc, weights, reps, hop):
        for way in range(2):
            def both(way=way):
                for r in reps:
                    fold(acc, weights, r, at_hop(way, hop))
            on(arrives(way, hop), both)

    gate_acc[...] = jnp.zeros_like(gate_acc)
    up_acc[...] = jnp.zeros_like(up_acc)
    for r in range(n_rep):
        fold(gate_acc, gate_all, r, fs)
        fold(up_acc, up_all, r, fs)

    def ffn_step(hop, carry):
        on(hop > 1, lambda: pump(GATE, hop))
        fold_hop(gate_acc, gate_all, [rep], hop)

        def late_up():
            rep_wait(UP, hop - 1)
            fold_hop(up_acc, up_all, others(), hop - 1)

        on(hop > 1, late_up)
        on(hop > 1, lambda: pump(UP, hop))

        def start_down():
            begin(DOWN_A)
            begin(DOWN_B)

        on(hop == last_hop - 1, start_down)
        fold_hop(up_acc, up_all, [rep], hop)
        rep_wait(GATE, hop)
        fold_hop(gate_acc, gate_all, others(), hop)
        return carry

    lax.fori_loop(1, last_hop + 1, ffn_step, 0)
    rep_wait(UP, last_hop)
    fold_hop(up_acc, up_all, others(), last_hop)

    hid = hidden.shape[2]

    def hidden_chunk(i, carry):
        here = pl.ds(pl.multiple_of(i * chunk, chunk), chunk)
        for r in range(n_rep):
            a = gate_acc[r, here, :] * gate_scale_ref[:, r * hid:(r + 1) * hid]
            b = up_acc[r, here, :] * up_scale_ref[:, r * hid:(r + 1) * hid]
            hidden[r, here, :] = (a / (1.0 + jnp.exp(-a)) * b).astype(jnp.bfloat16)
        return carry

    lax.fori_loop(0, chunks, hidden_chunk, 0)
    ffn_acc[...] = jnp.zeros_like(ffn_acc)

    def fold_down(r, f):
        def body(i, carry):
            here = pl.ds(pl.multiple_of(i * chunk, chunk), chunk)
            term = jnp.dot(hidden[r, here, :], down_all[r, f], preferred_element_type=jnp.float32)
            ffn_acc[f, here, :] = ffn_acc[f, here, :] + term
            return carry

        lax.fori_loop(0, chunks, body, 0)

    def part_copy(f, owner, sender):
        sub = lax.rem(f, per_own)
        return pltpu.make_async_remote_copy(
            src_ref=part.at[f], dst_ref=parts_in.at[sender, sub], send_sem=part_send.at[f],
            recv_sem=part_recv.at[sender, sub], device_id={"tp": owner}, device_id_type=MESH)

    def finish(f):
        def body(i, carry):
            here = pl.ds(pl.multiple_of(i * chunk, chunk), chunk)
            part[f, here, :] = (ffn_acc[f, here, :] * scale_all[f, 1]).astype(jnp.bfloat16)
            return carry

        lax.fori_loop(0, chunks, body, 0)
        owner = f // per_own
        on(owner != tp, lambda: part_copy(f, owner, tp).start())

    def down_own(hop):
        for way in range(2):
            on(arrives(way, hop), lambda way=way: fold_down(rep, at_hop(way, hop)))

    def down_others(hop):
        rep_wait(DOWN_B, hop)
        for way in range(2):
            def close(way=way):
                for r in others():
                    fold_down(r, at_hop(way, hop))
                finish(at_hop(way, hop))
            on(arrives(way, hop), close)

    pump(DOWN_A, 1)
    for r in range(n_rep):
        fold_down(r, fs)
    finish(fs)

    def down_step(hop, carry):
        on(hop > 1, lambda: pump(DOWN_A, hop))
        on(hop > 1, lambda: down_others(hop - 1))
        pump(DOWN_B, hop)
        down_own(hop)
        rep_wait(DOWN_A, hop)
        return carry

    lax.fori_loop(1, last_hop + 1, down_step, 0)
    down_others(last_hop)

    for k in range(1, n_tp):
        sender = lax.rem(tp + k, n_tp)
        for sub in range(per_own):
            part_copy(tp * per_own + sub, tp, sender).wait_recv()

    def close_span(i, carry):
        here = pl.ds(pl.multiple_of(i * chunk, chunk), chunk)
        for sub in range(per_own):
            cols = slice(sub * block, (sub + 1) * block)
            total = part[tp * per_own + sub, here, :].astype(jnp.float32)
            for k in range(1, n_tp):
                total += parts_in[lax.rem(tp + k, n_tp), sub, here, :].astype(jnp.float32)
            total = total.astype(jnp.bfloat16).astype(jnp.float32)
            kept = tok_all[tp, here, cols].astype(jnp.float32)
            result_ref[here, cols] = (kept + total).astype(jnp.bfloat16)
        return carry

    lax.fori_loop(0, chunks, close_span, 0)

    for kind in range(KINDS):
        for way in range(2):
            def sent(hop, carry, kind=kind, way=way):
                on(leaves(way, hop), lambda: send(kind, way, hop).wait_send())
                if kind != SCALES:
                    def rep_sent():
                        for k in range(1, n_rep):
                            rep_copy(kind, way, hop, k, rep).wait_send()
                    on(arrives(way, hop), rep_sent)
                return carry

            lax.fori_loop(1, last_hop + 1, sent, 0)
    for kind in (OUT_ROWS, GATED):
        for k in range(1, n_tp):
            tp_copy(kind, k, tp).wait_send()

    def part_sent(f, carry):
        owner = f // per_own
        on(owner != tp, lambda: part_copy(f, owner, tp).wait_send())
        return carry

    lax.fori_loop(0, n_fs, part_sent, 0)


def shards(
    sizes,
    tokens,
    pre_gain,
    u_weight,
    u_scale,
    v_weight,
    v_scale,
    group_gain,
    span_weight,
    span_bias,
    out_weight,
    out_scale,
    ffn_gain,
    gate_weight,
    gate_scale,
    up_weight,
    up_scale,
    down_weight,
    down_scale,
):
    n_rep, n_fs, n_tp = sizes
    bf16, f32 = jnp.bfloat16, jnp.float32

    def halves(array, axis):
        shape = array.shape
        split = shape[:axis] + (n_rep, shape[axis] // n_rep) + shape[axis + 1:]
        return jnp.moveaxis(array.astype(bf16).reshape(split), axis, 0)

    rows, own_width = tokens.shape
    block, local_hidden = gate_weight.shape
    hid = local_hidden // n_rep
    channels = u_weight.shape[1]
    groups, span = span_weight.shape[0], span_weight.shape[1]
    uv = halves(jnp.stack([u_weight, v_weight]), 1)
    bias = jnp.repeat(jnp.transpose(span_bias), channels // groups, axis=1)
    row = lambda vector: vector.reshape(1, -1)
    operands = (
        tokens, row(out_scale), row(down_scale), uv, halves(out_weight, 0), halves(gate_weight, 1), halves(up_weight, 1),
        halves(down_weight, 0), row(pre_gain), row(ffn_gain), row(u_scale), row(v_scale),
        row(group_gain), span_weight, bias, row(gate_scale),
        row(up_scale),
    )
    hbm, vmem = pl.BlockSpec(memory_space=pl.ANY), pl.BlockSpec(memory_space=pltpu.VMEM)
    per_own = own_width // block
    steps = n_fs - 1
    return pl.pallas_call(
        functools.partial(layer_kernel, sizes),
        out_shape=jax.ShapeDtypeStruct((rows, own_width), bf16),
        in_specs=[hbm] * 8 + [vmem] * 9,
        out_specs=vmem,
        scratch_shapes=[
            pltpu.VMEM((n_tp, rows, own_width), bf16),
            pltpu.VMEM((n_fs, 2, 1, block), f32),
            pltpu.VMEM((n_fs, 2, block, channels), bf16),
            pltpu.VMEM((n_fs, n_tp, channels, block), bf16),
            pltpu.VMEM((n_rep, n_fs, block, hid), bf16),
            pltpu.VMEM((n_rep, n_fs, block, hid), bf16),
            pltpu.VMEM((n_rep, n_fs, hid, block), bf16),
            pltpu.VMEM((n_fs, rows, block), bf16),
            pltpu.VMEM((n_tp, rows, channels), bf16),
            pltpu.VMEM((n_rep, rows, hid), f32),
            pltpu.VMEM((n_rep, rows, hid), f32),
            pltpu.VMEM((n_rep, rows, hid), bf16),
            pltpu.VMEM((n_fs, rows, block), f32),
            pltpu.VMEM((n_fs, rows, block), bf16),
            pltpu.VMEM((n_tp, per_own, rows, block), bf16),
            pltpu.SemaphoreType.DMA((3 + 6 * n_rep,)),
            pltpu.SemaphoreType.DMA((KINDS, 2, steps)),
            pltpu.SemaphoreType.DMA((KINDS, 2, steps)),
            pltpu.SemaphoreType.DMA((KINDS, 2, steps, n_rep - 1)),
            pltpu.SemaphoreType.DMA((KINDS, 2, steps, n_rep - 1)),
            pltpu.SemaphoreType.DMA((3, n_tp - 1)),
            pltpu.SemaphoreType.DMA((3, n_tp - 1)),
            pltpu.SemaphoreType.DMA((n_fs,)),
            pltpu.SemaphoreType.DMA((n_tp, per_own)),
        ],
        compiler_params=pltpu.CompilerParams(
            collective_id=0, has_side_effects=True, vmem_limit_bytes=62 * 1024 * 1024
        ),
    )(*operands)


def solution(mesh):
    placed = (
        P(("rep", "fs"), "tp"),
        P(),
        P("fs", "tp"),
        P("tp"),
        P("fs", "tp"),
        P("tp"),
        P("tp"),
        P("tp", None, None),
        P("tp", None),
        P("tp", "fs"),
        P("fs"),
        P(),
        P("fs", "tp"),
        P("tp"),
        P("fs", "tp"),
        P("tp"),
        P("tp", "fs"),
        P("fs"),
    )
    sizes = (mesh.shape["rep"], mesh.shape["fs"], mesh.shape["tp"])
    return jax.shard_map(
        functools.partial(shards, sizes), mesh=mesh, in_specs=placed, out_specs=P(("rep", "fs"), "tp"), check_vma=False
    )
```

time: 230 us -> 254 us (1.10)
  Pallas kernels: 212 us -> 233 us
    pallas_call x1, Pallas kernels: 212 us -> 233 us  [shards(): pl.pallas_call(functools.partial(layer_kernel, sizes), out_shape=jax.Shap...]
    convert_element_type x3 -> x0, local copies, waits for them, and re-layouts: 6.65 us -> none  [share(): lax.dynamic_slice_in_dim(array, rep * width, width, axis)]
    unnamed x3 -> x5, local copies, waits for them, and re-layouts: 1.87 us -> 6.03 us
    reshape x2 -> x4, local copies, waits for them, and re-layouts: 2.73 us -> 5.78 us  [the longest x2 3.16 us: halves(): return jnp.moveaxis(array.astype(bf16).reshape(split), axis, 0)]
where the time goes in v3:
time: 254 us; the launch traced here: 253 us
  Pallas kernels  233 us (92%)
  local copies, waits for them, and re-layouts  13.2 us (5%)
  other arithmetic  6.44 us (3%)
    pallas_call x1, Pallas kernels, shards(): pl.pallas_call(functools.partial(layer_kernel, sizes), out_shape=jax.Shap...  233 us
    unnamed x5, local copies, waits for them, and re-layouts  6.03 us

profile of v3, /device:TPU:0, one launch (start us, length us, event | category | flops | bytes accessed | tf_op | source)
XLA Modules:
  0.0 252.8 jit_solution(15197188092956432529)
XLA Ops:
  0.0 0.0 copy-start
  0.0 1.3 reshape.61.gate_scale_ref
  1.3 1.3 reshape.62.up_scale_ref
  2.6 0.7 broadcast_in_dim.3
  3.3 0.7 copy.24.bias_ref
  4.0 1.0 convert.8
  5.0 1.0 convert.9
  6.0 0.7 maximum_bitcast_fusion.uv_ref
  6.7 0.0 copy-done
  6.7 0.7 convert_element_type.14
  7.4 2.1 copy.20
  9.5 1.6 copy.21
  11.1 2.1 copy.22
  13.1 1.6 copy.23
  14.7 3.1 %convert_element_type.17 = bf16[1408,512]{1,0:T(8,128)(2,1)} convert(f32[1408,512]{1,0:T(8,128)} %param.34) | non-fusion elementwise | flops 720896 | bytes 4325376 | tf_op jit(solution)/shard_map/convert_element_type | solution.py:497
  17.8 233.1 %shard_map.172 = bf16[512,512]{1,0:T(8,128)(2,1)} custom-call(bf16[512,512]{1,0:T(8,128)(2,1)} %tokens_ref.1, f32[1,512]{1,0:T(1,128)} %bitcast.30, f32[1,512]{1,0:T(1,128)} %bitcast.31, bf16[2,2,256,128]{3,2,1,0:T(8,128)(2,1)} %maximum_bitcast_fusion.uv_ref, bf16[2,64,512]{2,1,0:T(8,128)(2,1)} %bitcast.24, bf16[2,512,704]{2,1,0:T(8,128)(2,1)} %bitcast.19, ...), custom_call_target="tpu_custom_call" | custom-call | tf_op jit(solution)/shard_map/pallas_call | solution.py:516
  251.0 1.9 copy.26
Async XLA Ops:
  0.0 6.7 %copy-start = (f32[128,512]{1,0:T(8,128)S(1)}, f32[128,512]{1,0:T(8,128)}, u32[]{:S(2)}) copy-start(f32[128,512]{1,0:T(8,128)} %param.27) | copy-start | bytes 786436
